TPU v7x, 512 devices: a whole 4x4x16 slice. The times are simulated.
512 devices in a mesh: sp: 32 (over z, core), tp: 16 (over y, x).
Axes of the slice: x: 4, y: 4, z: 16, core: 2. Of those that a mesh axis runs over, the one named last changes fastest.
Arguments:
- stream: bfloat16 [4096, 2048], P('sp'), may hold values from -6 to 6
- query_small: bfloat16 [4096, 1024], P('sp', 'tp'), may hold values from -6 to 6
- key_small: bfloat16 [4096, 1024], P('sp', 'tp'), may hold values from -6 to 6
- value_small: bfloat16 [4096, 1024], P('sp', 'tp'), may hold values from -6 to 6
- query_large: bfloat16 [4096, 2048], P('sp', 'tp'), may hold values from -6 to 6
- key_large: bfloat16 [4096, 2048], P('sp', 'tp'), may hold values from -6 to 6
- value_large: bfloat16 [4096, 2048], P('sp', 'tp'), may hold values from -6 to 6
- key_bias: bfloat16 [4096, 2, 16], P('sp', None, 'tp'), may hold values from -16 to 1
- out_small: bfloat16 [1024, 2048], P('tp'), may hold values from -0.75 to 0.75
- out_large: bfloat16 [2048, 2048], P('tp'), may hold values from -0.75 to 0.75
- gain_one: float32 [2048], replicated, may hold values from 0.1 to 1.9
- shift_one: float32 [2048], replicated, may hold values from -1.5 to 1.5
- gain_two: float32 [2048], replicated, may hold values from 0.1 to 1.9
- shift_two: float32 [2048], replicated, may hold values from -1.5 to 1.5
- expert_pick: int32 [4096, 2], P('sp'), may hold values from 0 to 31, as said below
- route_weight: float32 [4096, 2], P('sp'), may hold values from 0.2 to 1
- w_gate: bfloat16 [32, 2048, 4096], P('sp', None, 'tp'), may hold values from -0.125 to 0.125
- w_up: bfloat16 [32, 2048, 4096], P('sp', None, 'tp'), may hold values from -0.125 to 0.125
- w_down: bfloat16 [32, 4096, 2048], P('sp', 'tp'), may hold values from -0.09375 to 0.09375
Outputs:
- result: bfloat16 [4096, 2048], P(('sp', 'tp'))
Inputs may be any that keep to these rules, and one draw needn't show every extreme that they name: In each aligned block of 128 positions (the positions of one index of sp), no expert is named more than 16 times, and in every block some expert is named exactly 16 times. The two experts of a position differ and lie in one group: equal values of expert_pick // 8.
All inputs are finite; a program needn't handle non-finite values.
Results may differ from a plain program's by a relative error of at most 0.017.
Values may be sent and summed in bfloat16 or wider, within the bound.
No kernel may reach another device: no remote copies, remote signals or barrier semaphores. Data moves between devices by JAX's collectives and lax.ppermute only.
A program may use at most 64 MiB of HBM per device.

v0:
```python
import jax
import jax.numpy as jnp
from jax import lax
from jax.sharding import Mesh
from jax.sharding import PartitionSpec as P

HEAD_SMALL = 64
HEAD_LARGE = 128
SP = ("sp_0", "sp_1")
SP_TP = ("sp_0", "sp_1", "tp")


ALPHA_RES = 2.0**0.25
NORM_EPS = 1e-05


def in_one_piece(arrays, axis, dim, along):
    columns = [a.reshape(*a.shape[:along], -1) for a in arrays]
    both = jnp.concatenate(columns, axis=along)
    whole, at, done = (lax.all_gather(both, axis, axis=dim, tiled=True), 0, [])
    for a, column in zip(arrays, columns):
        slab = whole[..., at : at + column.shape[along]]
        done.append(slab.reshape(*slab.shape[:along], *a.shape[along:]))
        at += column.shape[along]
    return tuple(done)


def over_pieces(shard, axis):
    blocks = lax.all_gather(shard, axis).astype(jnp.float32)
    return blocks.sum(axis=0)


def cut_along(shard, dim, length):
    shape = shard.shape
    blocks = shard.reshape(*shape[:dim], length, shape[dim] // length, *shape[dim + 1 :])
    return jnp.moveaxis(blocks, dim, 0)


def joined_along(blocks, dim):
    blocks = jnp.moveaxis(blocks, 0, dim)
    shape = blocks.shape
    return blocks.reshape(*shape[:dim], shape[dim] * shape[dim + 1], *shape[dim + 2 :])


def turned_blocks(blocks, axes, sequence):
    shape = [lax.axis_size(a) for a in axes]
    blocks = blocks.reshape(*shape, *blocks.shape[1:])
    for k in sequence:
        blocks = lax.all_to_all(blocks, axes[k], split_axis=k, concat_axis=k, tiled=True)
    return blocks.reshape(-1, *blocks.shape[len(axes) :])


def core_and_chips(shard, groups, sequence, split_dim, concat_dim):
    length = lax.axis_size(groups[0]) * lax.axis_size(groups[1])
    blocks = cut_along(shard, split_dim, length)
    return joined_along(turned_blocks(blocks, groups, sequence), concat_dim)


def from_everyone(shard, axis):
    length = lax.axis_size(axis)
    return lax.all_to_all(
        jnp.broadcast_to(shard[None], (length, *shard.shape)), axis, 0, 0, tiled=True
    )


def collect(shard, axis, dim):
    blocks = from_everyone(shard, axis)
    return joined_along(blocks, dim)


def summed_on_arrival(shard, axis, dim):
    blocks = cut_along(shard, dim, lax.axis_size(axis))
    arrived = lax.all_to_all(blocks, axis, split_axis=0, concat_axis=0, tiled=True)
    return arrived.astype(jnp.float32).sum(axis=0)


def layer_norm(inputs, gain_vec, shift_vec):
    average = jnp.mean(inputs, axis=-1, keepdims=True)
    centred = inputs - average
    variance = jnp.mean(centred * centred, axis=-1, keepdims=True)
    return centred * lax.rsqrt(variance + NORM_EPS) * gain_vec + shift_vec


def stick_group(queries, key_rows, value_rows, log_bias, position):
    query_count = queries.shape[0]
    head_count = queries.shape[1]
    value_size = value_rows.shape[2]
    key_span = 4 * query_count
    score_scale = queries.shape[2] ** (-0.5)
    query_pos = position * query_count + jnp.arange(query_count, dtype=jnp.int32)
    block_count = (position * query_count + query_count + key_span - 1) // key_span

    def visit_block(turn_index, carry):
        running, stay_sum = carry
        first_key = (block_count - 1 - turn_index) * key_span
        key_block = lax.dynamic_slice_in_dim(key_rows, first_key, key_span, 0)
        value_block = lax.dynamic_slice_in_dim(value_rows, first_key, key_span, 0)
        bias_block = lax.dynamic_slice_in_dim(log_bias, first_key, key_span, 0).astype(jnp.float32)
        scores = jnp.einsum("qhd,khd->hqk", queries, key_block, preferred_element_type=jnp.float32)
        scores = scores * score_scale + bias_block.T[:, None, :]
        key_pos = first_key + jnp.arange(key_span, dtype=jnp.int32)
        causal = (key_pos[None, :] < query_pos[:, None])[None]
        log_stay = jnp.where(causal, jax.nn.log_sigmoid(-scores), 0.0)
        later_sum = lax.cumsum(log_stay, axis=2, reverse=True) - log_stay + stay_sum[:, :, None]
        stick_weight = jnp.where(
            causal, jnp.exp(jax.nn.log_sigmoid(scores) + later_sum), 0.0
        ).astype(jnp.bfloat16)
        running = running + jnp.einsum(
            "hqk,khd->qhd", stick_weight, value_block, preferred_element_type=jnp.float32
        )
        stay_sum = stay_sum + jnp.sum(log_stay, axis=2)
        return (running, stay_sum)

    start_total = jnp.zeros((query_count, head_count, value_size), jnp.float32)
    start_stay = jnp.zeros((head_count, query_count), jnp.float32)
    running, stay_sum = lax.fori_loop(0, block_count, visit_block, (start_total, start_stay))
    return running.reshape(query_count, head_count * value_size).astype(jnp.bfloat16)


def split_heads(array, head_size):
    return array.reshape(array.shape[0], array.shape[1] // head_size, head_size)


def local(
    stream,
    query_small,
    key_small,
    value_small,
    query_large,
    key_large,
    value_large,
    key_bias,
    out_small,
    out_large,
    gain_one,
    shift_one,
    gain_two,
    shift_two,
    expert_pick,
    route_weight,
    w_gate,
    w_up,
    w_down,
):
    row_count = stream.shape[0]
    position = lax.axis_index(SP)
    gathered = in_one_piece((key_small, value_small, key_large, value_large, key_bias), SP, 0, 1)
    att_small = stick_group(
        split_heads(query_small, HEAD_SMALL),
        split_heads(gathered[0], HEAD_SMALL),
        split_heads(gathered[1], HEAD_SMALL),
        gathered[4][:, 0],
        position,
    )
    att_large = stick_group(
        split_heads(query_large, HEAD_LARGE),
        split_heads(gathered[2], HEAD_LARGE),
        split_heads(gathered[3], HEAD_LARGE),
        gathered[4][:, 1],
        position,
    )
    partial_value = jnp.dot(att_small, out_small, preferred_element_type=jnp.float32)
    partial_value = partial_value + jnp.dot(
        att_large, out_large, preferred_element_type=jnp.float32
    )
    mixer_out = over_pieces(partial_value.astype(jnp.bfloat16), "tp").astype(jnp.float32)
    normed = layer_norm(
        ALPHA_RES * stream.astype(jnp.float32) + mixer_out, gain_one, shift_one
    ).astype(jnp.bfloat16)
    experts = w_gate.shape[0] * lax.axis_size(SP)
    capacity = 4 * row_count // experts
    tp_count = lax.axis_size("tp")
    tp_index = lax.axis_index("tp")
    per_lane = capacity // tp_count
    flat_picks = expert_pick.reshape(-1)
    one_hot = (flat_picks[:, None] == jnp.arange(experts, dtype=jnp.int32)[None, :]).astype(
        jnp.int32
    )
    slot_rank = jnp.sum((jnp.cumsum(one_hot, axis=0) - one_hot) * one_hot, axis=1)
    slot_index = (flat_picks * capacity + slot_rank).reshape(row_count, 2)
    target = (
        jnp.arange(experts, dtype=jnp.int32)[:, None] * capacity
        + tp_index * per_lane
        + jnp.arange(per_lane, dtype=jnp.int32)[None, :]
    ).reshape(-1)
    own_select = [target[:, None] == slot_index[None, :, pick_index] for pick_index in range(2)]
    placing = (own_select[0] | own_select[1]).astype(jnp.bfloat16)
    outgoing = jnp.dot(placing, normed, preferred_element_type=jnp.float32).astype(jnp.bfloat16)
    arrived = core_and_chips(
        outgoing.reshape(experts, per_lane, normed.shape[1]), ("sp_0", "sp_1"), (1, 0), 0, 0
    )
    piece_rows = collect(arrived, "tp", 1)
    flat_rows = piece_rows.reshape(-1, piece_rows.shape[2])
    gate = jnp.dot(flat_rows, w_gate[0], preferred_element_type=jnp.float32)
    upper = jnp.dot(flat_rows, w_up[0], preferred_element_type=jnp.float32)
    hidden = (jax.nn.silu(gate) * upper).astype(jnp.bfloat16)
    expert_terms = jnp.dot(hidden, w_down[0], preferred_element_type=jnp.float32).reshape(
        piece_rows.shape
    )
    summed = summed_on_arrival(expert_terms.astype(jnp.bfloat16), "tp", 1).astype(jnp.bfloat16)
    returned = lax.all_to_all(summed, SP, split_axis=0, concat_axis=0, tiled=True).reshape(
        experts * per_lane, normed.shape[1]
    )
    picked_first = jnp.einsum(
        "sr,sd->rd",
        own_select[0].astype(jnp.bfloat16),
        returned,
        preferred_element_type=jnp.float32,
    )
    picked_second = jnp.einsum(
        "sr,sd->rd",
        own_select[1].astype(jnp.bfloat16),
        returned,
        preferred_element_type=jnp.float32,
    )
    partial_mix = route_weight[:, 0:1] * picked_first + route_weight[:, 1:2] * picked_second
    expert_mix = summed_on_arrival(partial_mix.astype(jnp.bfloat16), "tp", 0)
    own_count = row_count // tp_count
    own_rows = lax.dynamic_slice_in_dim(normed, tp_index * own_count, own_count, 0).astype(
        jnp.float32
    )
    return layer_norm(ALPHA_RES * own_rows + expert_mix, gain_two, shift_two).astype(jnp.bfloat16)


def solution(mesh):
    torus = Mesh(mesh.devices.reshape(16, 2, mesh.shape["tp"]), ("sp_0", "sp_1", "tp"))
    in_specs = (
        P(SP, None),
        P(SP, "tp"),
        P(SP, "tp"),
        P(SP, "tp"),
        P(SP, "tp"),
        P(SP, "tp"),
        P(SP, "tp"),
        P(SP, None, "tp"),
        P("tp", None),
        P("tp", None),
        P(),
        P(),
        P(),
        P(),
        P(SP, None),
        P(SP, None),
        P(SP, None, "tp"),
        P(SP, None, "tp"),
        P(SP, "tp", None),
    )
    out_specs = P(SP_TP, None)
    return jax.shard_map(local, mesh=torus, in_specs=in_specs, out_specs=out_specs, check_vma=False)
```

profile of v0, /device:TPU:1, one launch (start us, length us, event | category | flops | bytes accessed | tf_op | source)
XLA Modules:
  0.0 385.1 jit_solution(1701489663593663720)
XLA Ops:
  6.5 0.9 copy.99
  7.4 0.8 copy.100
  8.2 0.8 copy.101
  9.1 1.5 concatenate.3
  10.7 79.1 %all-gather.4.cloned.1.call-done = bf16[4096,386]{1,0:T(8,128)(2,1)} async-done(((bf16[128,386]{1,0:T(8,128)(2,1)}), bf16[4096,386]{1,0:T(8,128)(2,1)}) %all-gather.4.cloned.1.call-update) | async-done | bytes 3162128 | tf_op jit(solution)/shard_map/all_gather | solution.py:20
  89.8 1.4 slice_bitcast_fusion.6
  91.3 1.0 slice_reduce_fusion
  92.4 1.1 slice_bitcast_fusion.4
  93.5 3.2 while.31
  93.5 1.3 fusion.110
  94.8 1.1 fusion.111
  96.1 0.4 fusion.112
  96.5 0.2 fusion.113
  96.7 2.1 slice_bitcast_fusion.7
  98.8 1.1 copy.102
  99.9 0.3 copy.103
  100.3 3.1 while.30
  100.4 0.4 fusion.103
  100.8 1.1 fusion.104
  102.0 0.4 fusion.105
  102.4 1.0 fusion.106
  103.5 0.3 fusion.67
  103.8 1.2 fusion.46
  105.0 0.1 copy.104
  105.1 0.1 eq.58
  105.3 0.1 eq.54
  105.4 0.6 reduce-window.38
  106.0 0.2 slice_reduce_fusion.2
  106.2 0.1 fusion.61
  106.3 0.1 reduce_sum.105
  106.6 121.6 %all-gather.6.cloned.1.call-done = bf16[2048,2048]{1,0:T(8,128)(2,1)} async-done(((bf16[128,2048]{1,0:T(8,128)(2,1)}), bf16[2048,2048]{1,0:T(8,128)(2,1)}) %all-gather.6.cloned.1.call-update) | async-done | bytes 8388624 | tf_op jit(solution)/shard_map/all_gather | solution.py:29
  228.2 5.4 %convert_reduce_fusion = f32[128,2048]{1,0:T(8,128)S(1)} fusion(bf16[16,128,2048]{2,1,0:T(8,128)(2,1)} %bitcast.216), kind=kLoop, calls=%fused_computation.68 | loop fusion | flops 8126464 | bytes 9437184 | tf_op jit(solution)/shard_map/reduce_sum | solution.py:30
  233.6 0.2 fusion.54
  233.9 0.3 multiply_reduce_fusion
  234.2 0.1 copy-done.6
  234.3 0.3 add_convert_fusion
  234.6 0.8 copy-done.3
  235.4 0.2 convolution_convert_fusion.1
  235.7 0.1 reshape_reshape_reshape.3
  235.8 4.3 %all_to_all.30 = bf16[16,2,1,1,2048]{4,0,3,2,1:T(8,128)(2,1)S(1)} all-to-all(bf16[16,2,1,1,2048]{4,0,3,2,1:T(8,128)(2,1)S(1)} %copy.108), channel_id=1, replica_groups=mesh['sp_0'=16,'sp_1'=2,'tp'=16] {'sp_1'}, dimensions={1} | all-to-all | bytes 262144 | tf_op jit(solution)/shard_map/all_to_all | solution.py:49
  240.2 0.1 copy.109
  240.3 23.9 %all_to_all.31 = bf16[16,2,1,1,2048]{4,1,3,2,0:T(2,128)(2,1)S(1)} all-to-all(bf16[16,2,1,1,2048]{4,1,3,2,0:T(2,128)(2,1)S(1)} %copy.109), channel_id=1, replica_groups=mesh['sp_0'=16,'sp_1'=2,'tp'=16] {'sp_0'}, dimensions={0} | all-to-all | bytes 262144 | tf_op jit(solution)/shard_map/all_to_all | solution.py:49
  264.3 0.2 broadcast_in_dim.24
  264.5 29.5 %all_to_all.32 = bf16[16,32,1,2048]{3,1,2,0:T(8,128)(2,1)S(1)} all-to-all(bf16[16,32,1,2048]{3,1,2,0:T(8,128)(2,1)S(1)} %broadcast_in_dim.24), channel_id=1, replica_groups=mesh['sp_0'=16,'sp_1'=2,'tp'=16] {'tp'}, dimensions={0} | all-to-all | bytes 4194304 | tf_op jit(solution)/shard_map/all_to_all | solution.py:61
  294.0 1.2 copy.110
  295.3 0.7 fusion.52
  296.0 0.5 copy-done.13
  296.4 0.7 fusion.49
  297.2 0.7 fusion.44
  297.9 1.2 copy.111
  299.1 27.5 %all_to_all.33 = bf16[16,32,1,2048]{3,1,2,0:T(8,128)(2,1)S(1)} all-to-all(bf16[16,32,1,2048]{3,1,2,0:T(8,128)(2,1)S(1)} %copy.111), channel_id=1, replica_groups=mesh['sp_0'=16,'sp_1'=2,'tp'=16] {'tp'}, dimensions={0} | all-to-all | bytes 4194304 | tf_op jit(solution)/shard_map/all_to_all | solution.py:73
  326.5 0.4 reduce_sum.106
  326.9 0.5 broadcast.188
  327.4 0.7 reduce.16
  328.1 0.7 reshape.334
  328.8 14.7 %all-to-all-start.4 = ((bf16[32,2,1024]{2,1,0:T(2,128)(2,1)}), bf16[32,2,1024]{2,1,0:T(2,128)(2,1)S(1)}, u32[]{:S(2)}, u32[]{:S(2)}) async-start(bf16[32,2,1024]{2,1,0:T(2,128)(2,1)} %reshape.334), calls=%async_computation.4 | async-start | bytes 262144 | tf_op jit(solution)/shard_map/all_to_all | solution.py:201
  343.6 15.8 %all-to-all-done.4 = bf16[32,2,1024]{2,1,0:T(2,128)(2,1)S(1)} async-done(((bf16[32,2,1024]{2,1,0:T(2,128)(2,1)}), bf16[32,2,1024]{2,1,0:T(2,128)(2,1)S(1)}, u32[]{:S(2)}, u32[]{:S(2)}) %all-to-all-start.4) | async-done | bytes 131104 | tf_op jit(solution)/shard_map/all_to_all | solution.py:201
  359.5 0.4 convolution_multiply_fusion.3
  359.9 1.2 fusion.48
  361.2 3.6 all-to-all-start.5
  364.8 10.1 %all-to-all-done.5 = bf16[16,8,2048]{2,1,0:T(8,128)(2,1)S(1)} async-done(((bf16[16,8,2048]{2,1,0:T(8,128)(2,1)}), bf16[16,8,2048]{2,1,0:T(8,128)(2,1)S(1)}, u32[]{:S(2)}, u32[]{:S(2)}) %all-to-all-start.5) | async-done | bytes 524320 | tf_op jit(solution)/shard_map/all_to_all | solution.py:73
  374.9 0.9 fusion.70
  375.8 1.0 multiply_reduce_fusion.1
  376.8 1.5 add_convert_fusion.1
  (71 shorter events, 0.9 us)
Async XLA Ops:
  6.5 290.6 %copy-start = (bf16[1,256,2048]{2,1,0:T(8,128)(2,1)S(1)}, bf16[1,256,2048]{2,1,0:T(8,128)(2,1)}, u32[]{:S(2)}) copy-start(bf16[1,256,2048]{2,1,0:T(8,128)(2,1)} %param.41) | copy-start | bytes 3145732
  6.5 83.3 %all-gather.4.cloned.1.call-start = ((), (), s32[]{:S(2)}) async-start(), calls=%async_computation.6 | async-start | bytes 4325376 | tf_op jit(solution)/shard_map/all_gather | solution.py:20
  10.6 217.6 %all-gather.6.cloned.1.call-start = ((), (), s32[]{:S(2)}) async-start(), calls=%async_computation.7 | async-start | bytes 8912896 | tf_op jit(solution)/shard_map/all_gather | solution.py:29
  89.8 2.5 copy-start.1
  92.3 1.1 copy-start.14
  98.8 1.5 copy-start.15
  100.3 3.2 copy-start.5
  100.3 3.5 copy-start.4
  103.5 1.6 copy-start.10
  228.2 5.4 %copy-start.2 = (bf16[128,2048]{1,0:T(8,128)(2,1)S(1)}, bf16[128,2048]{1,0:T(8,128)(2,1)}, u32[]{:S(2)}) copy-start(bf16[128,2048]{1,0:T(8,128)(2,1)} %param.23) | copy-start | bytes 1572868
  233.6 0.7 copy-start.6
  233.6 0.7 copy-start.7
  234.6 0.8 copy-start.3
  294.0 1.2 copy-start.12
  295.2 1.2 copy-start.13
  326.5 17.0 %copy-start.11 = (f32[128,2]{0,1:T(2,128)S(1)}, f32[128,2]{0,1:T(2,128)}, u32[]{:S(2)}) copy-start(f32[128,2]{0,1:T(2,128)} %param.38) | copy-start | bytes 3076
  328.8 30.6 %all-to-all-start.4 = ((bf16[32,2,1024]{2,1,0:T(2,128)(2,1)}), bf16[32,2,1024]{2,1,0:T(2,128)(2,1)S(1)}, u32[]{:S(2)}, u32[]{:S(2)}) async-start(bf16[32,2,1024]{2,1,0:T(2,128)(2,1)} %reshape.334), calls=%async_computation.4 | async-start | bytes 262144 | tf_op jit(solution)/shard_map/all_to_all | solution.py:201
  359.5 17.3 %copy-start.8 = (f32[2048]{0:T(1024)S(1)}, f32[2048]{0:T(1024)}, u32[]{:S(2)}) copy-start(f32[2048]{0:T(1024)} %param.36) | copy-start | bytes 24580
  359.5 17.3 %copy-start.9 = (f32[2048]{0:T(1024)S(1)}, f32[2048]{0:T(1024)}, u32[]{:S(2)}) copy-start(f32[2048]{0:T(1024)} %param.35) | copy-start | bytes 24580
  361.2 13.7 %all-to-all-start.5 = ((bf16[16,8,2048]{2,1,0:T(8,128)(2,1)}), bf16[16,8,2048]{2,1,0:T(8,128)(2,1)S(1)}, u32[]{:S(2)}, u32[]{:S(2)}) async-start(bf16[16,8,2048]{2,1,0:T(8,128)(2,1)} %fusion.48), calls=%async_computation.5 | async-start | bytes 1048576 | tf_op jit(solution)/shard_map/all_to_all | solution.py:73
Sparse Core Ops, SparseCore 0:
  10.7 79.0 all-gather.3
  105.1 123.0 all-gather.5
where the time goes:
time: 386 us; the launch traced here: 385 us
  waiting for transfers between devices  227 us (59%)
  blocking collectives  85.2 us (22%)
  starting transfers between devices  18.3 us (5%)
  local copies, waits for them, and re-layouts  17.8 us (5%)
  other arithmetic  14.6 us (4%)
  between operations  13.8 us (4%)
  matrix products  8.43 us (2%)
    all_gather x1, waiting for transfers between devices, over_pieces(): blocks = lax.all_gather(shard, axis).astype(jnp.float32)  122 us
    all_gather x1, waiting for transfers between devices, in_one_piece(): whole, at, done = (lax.all_gather(both, axis, axis=dim, tiled=True), 0, [])  79.1 us
    all_to_all x1, blocking collectives, from_everyone(): lax.all_to_all(jnp.broadcast_to(shard[None], (length, *shard.shape)), axi...  29.5 us
    all_to_all x2, blocking collectives, turned_blocks(): lax.all_to_all(blocks, axes[k], split_axis=k, concat_axis=k, tiled=True)  28.2 us
    all_to_all x1, blocking collectives, summed_on_arrival(): lax.all_to_all(blocks, axis, split_axis=0, concat_axis=0, tiled=True)  27.5 us
    all_to_all x1, waiting for transfers between devices, local(): lax.all_to_all(summed, SP, split_axis=0, concat_axis=0, tiled=True)  15.8 us
    all_to_all x1, starting transfers between devices, local(): lax.all_to_all(summed, SP, split_axis=0, concat_axis=0, tiled=True)  14.7 us
    all_to_all x1, waiting for transfers between devices, summed_on_arrival(): lax.all_to_all(blocks, axis, split_axis=0, concat_axis=0, tiled=True)  10.1 us
  transfers between devices with their start and end apart: 4, of which 4 were waited for; matrix products, arithmetic and copies ran while one was open for 0% of the time, Pallas kernels for 0%

commit v1 on v0

v1 whole, which is shorter than its diff:
```python
import jax
import jax.numpy as jnp
from jax import lax
from jax.experimental import pallas as pl
from jax.experimental.pallas import tpu as pltpu
from jax.sharding import Mesh
from jax.sharding import PartitionSpec as P

SP = ("a", "b", "c")
TP = ("y", "x")
ALPHA_RES = 2.0**0.25
NORM_EPS = 1e-05
BF16 = jnp.bfloat16
F32 = jnp.float32


def call(body, out_shape, *args, scratch=(), name=None):
    return pl.pallas_call(
        body,
        out_shape=out_shape,
        scratch_shapes=list(scratch),
        compiler_params=pltpu.CompilerParams(vmem_limit_bytes=48 * 1024 * 1024),
        name=name,
    )(*args)


def contract(lhs, rhs, dims):
    return lax.dot_general(lhs, rhs, (dims, ((), ())), preferred_element_type=F32)


def pack_body(ks, vs, kl, vl, qs, ql, bias, kv_out, q_out):
    for i in range(kv_out.shape[0]):
        kv_out[i, 0:128, 0:64] = ks[...]
        kv_out[i, 0:128, 64:128] = vs[...]
        kv_out[i, 0:128, 128:256] = kl[...]
        kv_out[i, 0:128, 256:384] = vl[...]
        kv_out[i, 128:144, :] = bias[...]
    q_out[:, 0:64] = qs[...]
    q_out[:, 64:128] = jnp.zeros((128, 64), BF16)
    q_out[:, 128:256] = ql[...]


def gather_keys(own, other, kv, bias, c):
    for b in range(4):
        for core in range(2):
            block = jnp.where(c == core, own[b], other[b])
            row = (2 * b + core) * 128
            kv[pl.ds(row, 128), :] = block[0:128]
            bias[0:1, pl.ds(row, 128)] = block[128:144, 0:128].astype(F32)[0:1]
            bias[1:2, pl.ds(row, 128)] = block[128:144, 128:256].astype(F32)[0:1]


def stick_tile(q, k, v, bias, scale, later, carry, mask):
    acc, stay = carry
    s = contract(q, k, ((1,), (1,))) * scale + bias
    soft = jnp.log1p(jnp.exp(-jnp.abs(s)))
    log_take = jnp.minimum(s, 0.0) - soft
    log_stay = log_take - s
    if mask is not None:
        log_stay = jnp.where(mask, log_stay, 0.0)
    high = log_stay.astype(BF16)
    low = (log_stay - high.astype(F32)).astype(BF16)
    sums = contract(high, later, ((1,), (0,))) + contract(low, later, ((1,), (0,)))
    w = jnp.exp(log_take + sums + stay)
    if mask is not None:
        w = jnp.where(mask, w, 0.0)
    acc = acc + contract(w.astype(BF16), v, ((1,), (0,)))
    stay = stay + sums[:, 0:1] + log_stay[:, 0:1]
    return acc, stay


def stick_rows(q, kv, bias, row_pos):
    rows = q.shape[0]
    width = 256
    j = lax.broadcasted_iota(jnp.int32, (width, width), 0)
    i = lax.broadcasted_iota(jnp.int32, (width, width), 1)
    later = jnp.where(j > i, 1.0, 0.0).astype(BF16)
    carry = [
        (jnp.zeros((rows, 128), F32), jnp.zeros((rows, 1), F32)),
        (jnp.zeros((rows, 128), F32), jnp.zeros((rows, 1), F32)),
    ]
    for block in reversed(range(4)):
        at = block * width
        mask = None
        if row_pos is not None:
            r = lax.broadcasted_iota(jnp.int32, (rows, width), 0) + row_pos
            mask = lax.broadcasted_iota(jnp.int32, (rows, width), 1) + at < r
        keys = kv[at : at + width, :]
        carry[0] = stick_tile(
            q[:, 0:128], keys[:, 0:128], keys[:, 0:128],
            bias[0:1, at : at + width], 64.0**-0.5, later, carry[0], mask,
        )
        carry[1] = stick_tile(
            q[:, 128:256], keys[:, 128:256], keys[:, 256:384],
            bias[1:2, at : at + width], 128.0**-0.5, later, carry[1], mask,
        )
    return carry


def with_stay(carry):
    (acc_s, stay_s), (acc_l, stay_l) = carry
    lane = lax.broadcasted_iota(jnp.int32, acc_s.shape, 1)
    high_s = stay_s.astype(BF16).astype(F32)
    high_l = stay_l.astype(BF16).astype(F32)
    head = jnp.where(lane == 0, high_s, jnp.where(lane == 1, stay_s - high_s, 0.0))
    head = jnp.where(lane == 2, high_l, jnp.where(lane == 3, stay_l - high_l, head))
    return jnp.where(lane < 64, head, acc_s), acc_l


def far_body(place, q1, q2, q3, own, other, o1, o2, o3, kv, bias, q):
    a = place[0]
    for n, ref in enumerate((q1, q2, q3)):
        q[n * 128 : (n + 1) * 128, :] = ref[...]

    @pl.when(a < 3)
    def _():
        gather_keys(own, other, kv, bias, place[1])
        first, second = with_stay(stick_rows(q[...], kv, bias, None))
        for n, ref in enumerate((o1, o2, o3)):
            ref[:, 0:128] = first[n * 128 : (n + 1) * 128].astype(BF16)
            ref[:, 128:256] = second[n * 128 : (n + 1) * 128].astype(BF16)

    @pl.when(a == 3)
    def _():
        for ref in (o1, o2, o3):
            ref[...] = jnp.zeros((128, 256), BF16)


def near_body(place, q, own, other, o, kv, bias):
    gather_keys(own, other, kv, bias, place[1])
    row_pos = (place[2] * 2 + place[1]) * 128
    first, second = with_stay(stick_rows(q[...], kv, bias, row_pos))
    o[:, 0:128] = first
    o[:, 128:256] = second


def project_body(o0, o1, o2, o3, w_small, w_large, out):
    att_s = o0[:, 0:128]
    att_l = o0[:, 128:256]
    stay_s = att_s[:, 0:1] + att_s[:, 1:2]
    stay_l = att_s[:, 2:3] + att_s[:, 3:4]
    for ref in (o1, o2, o3):
        part = ref[:, 0:128].astype(F32)
        att_s = att_s + jnp.exp(stay_s) * part
        att_l = att_l + jnp.exp(stay_l) * ref[:, 128:256].astype(F32)
        stay_s = stay_s + part[:, 0:1] + part[:, 1:2]
        stay_l = stay_l + part[:, 2:3] + part[:, 3:4]
    att_s = att_s[:, 64:128].astype(BF16)
    att_l = att_l.astype(BF16)
    for n in range(8):
        cols = slice(n * 256, (n + 1) * 256)
        part = contract(att_s, w_small[:, cols], ((1,), (0,)))
        part = (part + contract(att_l, w_large[:, cols], ((1,), (0,)))).astype(BF16)
        out[2 * n] = part[:, 0:128]
        out[2 * n + 1] = part[:, 128:256]


def route_body(place, arrived, stream, picks, u_out, slot_out, out):
    total = ALPHA_RES * stream[...].astype(F32)
    mixed = arrived[0].astype(F32)
    for n in range(1, 16):
        mixed = mixed + arrived[n].astype(F32)
    u = (total + mixed).astype(BF16)
    u_out[...] = u
    expert = lax.broadcasted_iota(jnp.int32, (32, 128), 0)
    hot0 = jnp.where(expert == picks[0:1, :], 1.0, 0.0)
    hot1 = jnp.where(expert == picks[1:2, :], 1.0, 0.0)
    j = lax.broadcasted_iota(jnp.int32, (128, 128), 0)
    i = lax.broadcasted_iota(jnp.int32, (128, 128), 1)
    before = jnp.where(j < i, 1.0, 0.0).astype(BF16)
    count = contract((hot0 + hot1).astype(BF16), before, ((1,), (0,)))
    rank0 = jnp.sum(hot0 * count, axis=0, keepdims=True).astype(jnp.int32)
    rank1 = jnp.sum(hot1 * count, axis=0, keepdims=True).astype(jnp.int32)
    slot0 = picks[0:1, :] * 16 + rank0
    slot1 = picks[1:2, :] * 16 + rank1
    slot_out[0:1, :] = slot0
    slot_out[1:2, :] = slot1
    slot = lax.broadcasted_iota(jnp.int32, (512, 128), 0)
    placing = jnp.where((slot == slot0) | (slot == slot1), 1.0, 0.0).astype(BF16)
    out[...] = contract(placing, u, ((1,), (0,))).astype(BF16)


def expert_body(
    place, rows, gain, shift, gate0, up0, down0, gate1, up1, down1, out, normed
):
    total = rows[0].astype(F32)
    for n in range(1, 16):
        total = total + rows[n].astype(F32)
    mean = jnp.sum(total, axis=-1, keepdims=True) * (1.0 / 2048)
    square = jnp.zeros(total.shape, F32)
    for n in range(16):
        centred = rows[n].astype(F32) - mean
        square = square + centred * centred
    rstd = lax.rsqrt(jnp.sum(square, axis=-1, keepdims=True) * (1.0 / 2048) + NORM_EPS)
    for n in range(16):
        cols = slice(n * 128, (n + 1) * 128)
        piece = (rows[n].astype(F32) - mean) * rstd * gain[:, cols] + shift[:, cols]
        piece = piece.astype(BF16).reshape(16, 2, 16, 128)
        normed[0, :, cols] = piece[:, 0].reshape(256, 128)
        normed[1, :, cols] = piece[:, 1].reshape(256, 128)
    c = place[1]
    for which, gate_w, up_w, down_w in ((c, gate0, up0, down0), (1 - c, gate1, up1, down1)):
        piece = normed[which]
        gate = contract(piece, gate_w[...], ((1,), (0,)))
        upper = contract(piece, up_w[...], ((1,), (0,)))
        hidden = (gate / (1.0 + jnp.exp(-gate)) * upper).astype(BF16)
        for n in range(8):
            term = contract(hidden, down_w[:, n * 256 : (n + 1) * 256], ((1,), (0,)))
            term = term.astype(BF16)
            out[2 * n, :, which] = term[:, 0:128].reshape(16, 16, 128)
            out[2 * n + 1, :, which] = term[:, 128:256].reshape(16, 16, 128)


def sum_body(arrived, out):
    total = arrived[0].astype(F32)
    for n in range(1, 16):
        total = total + arrived[n].astype(F32)
    out[...] = total.astype(BF16)


def mix_body(returned, slots, weight, u, out):
    slot = lax.broadcasted_iota(jnp.int32, (512, 128), 0)
    total = jnp.zeros((128, 128), F32)
    for k in range(2):
        placing = jnp.where(slot == slots[k : k + 1, :], 1.0, 0.0).astype(BF16)
        picked = contract(placing, returned[...], ((0,), (0,)))
        total = total + weight[:, k : k + 1] * picked
    out[:, :, 0:128] = u[...].reshape(16, 8, 128)
    out[:, :, 128:256] = total.astype(BF16).reshape(16, 8, 128)


def layer_norm(inputs, gain_vec, shift_vec):
    average = jnp.mean(inputs, axis=-1, keepdims=True)
    centred = inputs - average
    variance = jnp.mean(centred * centred, axis=-1, keepdims=True)
    return centred * lax.rsqrt(variance + NORM_EPS) * gain_vec + shift_vec


def final_body(arrived, gain1, shift1, gain2, shift2, out):
    u = jnp.concatenate([arrived[n, :, 0:128] for n in range(16)], axis=1).astype(F32)
    mix = jnp.concatenate([arrived[n, :, 128:256] for n in range(16)], axis=1).astype(F32)
    normed = layer_norm(u, gain1[...], shift1[...]).astype(BF16).astype(F32)
    out[...] = layer_norm(ALPHA_RES * normed + mix, gain2[...], shift2[...]).astype(BF16)


def shape(dims, dtype=BF16):
    return jax.ShapeDtypeStruct(dims, dtype)


def with_place(body, place, out_shape, *args, scratch=(), blocks=None):
    def whole(dims):
        return pl.BlockSpec(dims, lambda i, p, n=len(dims): (0,) * n)

    specs = [whole(arg.shape) for arg in args]
    for at, spec in (blocks or {}).items():
        specs[at] = spec
    outs = out_shape if isinstance(out_shape, list) else [out_shape]
    out_specs = [whole(o.shape) for o in outs]
    return pl.pallas_call(
        body,
        grid_spec=pltpu.PrefetchScalarGridSpec(
            num_scalar_prefetch=1,
            grid=(1,),
            in_specs=specs,
            out_specs=out_specs if isinstance(out_shape, list) else out_specs[0],
            scratch_shapes=list(scratch),
        ),
        out_shape=out_shape,
        compiler_params=pltpu.CompilerParams(vmem_limit_bytes=48 * 1024 * 1024),
    )(place, *args)


SWAP = ((0, 1), (1, 0))


def local(
    stream,
    query_small,
    key_small,
    value_small,
    query_large,
    key_large,
    value_large,
    key_bias,
    out_small,
    out_large,
    gain_one,
    shift_one,
    gain_two,
    shift_two,
    expert_pick,
    route_weight,
    w_gate,
    w_up,
    w_down,
):
    place = jnp.stack(
        [lax.axis_index(name) for name in ("a", "c", "b")] + [lax.axis_index(TP)]
    ).astype(jnp.int32)
    bias = key_bias.reshape(128, 2).T.reshape(1, 256)
    bias = jnp.broadcast_to(jnp.pad(bias, ((0, 0), (0, 128))), (16, 384))
    kv, q = call(
        pack_body,
        [shape((4, 144, 384)), shape((128, 256))],
        key_small, value_small, key_large, value_large, query_small, query_large, bias,
    )
    weights = (w_gate[0], w_up[0], w_down[0])
    q_far = [lax.ppermute(q, "a", [(i + d, i) for i in range(4 - d)]) for d in (1, 2, 3)]
    own = lax.all_to_all(kv, "b", 0, 0, tiled=True)
    other = lax.ppermute(own, "c", SWAP)
    keys = [pltpu.VMEM((1024, 384), BF16), pltpu.VMEM((8, 1024), F32)]
    far = with_place(
        far_body, place, [shape((128, 256))] * 3, *q_far, own, other,
        scratch=keys + [pltpu.VMEM((384, 256), BF16)],
    )
    back = [
        lax.ppermute(far[d - 1], "a", [(i, i + d) for i in range(4 - d)]) for d in (1, 2, 3)
    ]
    near = with_place(near_body, place, shape((128, 256), F32), q, own, other, scratch=keys)
    partial = call(project_body, shape((16, 128, 128)), near, *back, out_small, out_large)
    arrived = lax.all_to_all(partial, TP, 0, 0, tiled=True)
    u, slots, outgoing = with_place(
        route_body, place,
        [shape((128, 128)), shape((8, 128), jnp.int32), shape((512, 128))],
        arrived, stream, expert_pick.T,
        blocks={1: pl.BlockSpec((128, 128), lambda i, p: (0, p[3]))},
    )
    moved = lax.all_to_all(outgoing.reshape(16, 32, 128), ("a", "b"), 0, 0, tiled=True)
    rows = lax.all_to_all(
        jnp.broadcast_to(moved.reshape(1, 512, 128), (16, 512, 128)), TP, 0, 0, tiled=True
    )
    partner = [lax.ppermute(w, "c", SWAP) for w in weights]
    terms = with_place(
        expert_body, place, shape((16, 16, 2, 16, 128)),
        rows, gain_one.reshape(1, 2048), shift_one.reshape(1, 2048), *weights, *partner,
        scratch=[pltpu.VMEM((2, 256, 2048), BF16)],
    )
    summed = call(
        sum_body, shape((512, 128)),
        lax.all_to_all(terms.reshape(16, 512, 128), TP, 0, 0, tiled=True),
    )
    returned = lax.all_to_all(summed.reshape(16, 32, 128), ("a", "b"), 0, 0, tiled=True)
    mixed = call(
        mix_body, shape((16, 8, 256)), returned.reshape(512, 128), slots, route_weight, u
    )
    last = lax.all_to_all(mixed, TP, 0, 0, tiled=True)
    vectors = [v.reshape(1, 2048) for v in (gain_one, shift_one, gain_two, shift_two)]
    return call(final_body, shape((8, 2048)), last, *vectors)


def solution(mesh):
    torus = Mesh(mesh.devices.reshape(4, 4, 2, 4, 4), ("a", "b", "c", "y", "x"))
    in_specs = (
        P(SP, None),
        P(SP, TP),
        P(SP, TP),
        P(SP, TP),
        P(SP, TP),
        P(SP, TP),
        P(SP, TP),
        P(SP, None, TP),
        P(TP, None),
        P(TP, None),
        P(),
        P(),
        P(),
        P(),
        P(SP, None),
        P(SP, None),
        P(SP, None, TP),
        P(SP, None, TP),
        P(SP, TP, None),
    )
    out_specs = P(SP + TP, None)
    return jax.shard_map(local, mesh=torus, in_specs=in_specs, out_specs=out_specs, check_vma=False)
```

time: 386 us -> 222 us (0.58)
  waiting for transfers between devices: 227 us -> 45.7 us
  starting transfers between devices: 18.3 us -> 45.2 us
  Pallas kernels: 0 us -> 19.8 us
  other arithmetic: 14.6 us -> 0.08 us
  between operations: 13.8 us -> 0.27 us
  blocking collectives: 85.2 us -> 95.4 us
  matrix products: 8.43 us -> 0 us
  local copies, waits for them, and re-layouts: 17.8 us -> 11.8 us
    all_gather x2 -> x0, waiting for transfers between devices: 201 us -> none  [the longest x1 122 us: over_pieces(): blocks = lax.all_gather(shard, axis).astype(jnp.float32)]
    ppermute x0 -> x10, starting transfers between devices: none -> 31.2 us  [the longest x3 12.1 us: local(): lax.ppermute(far[d - 1], 'a', [(i, i + d) for i in range(4 - d)])]
    ppermute x0 -> x10, waiting for transfers between devices: none -> 21.8 us  [the longest x3 16.7 us: local(): lax.ppermute(q, 'a', [(i + d, i) for i in range(4 - d)])]
    pallas_call x0 -> x9, Pallas kernels: none -> 19.8 us  [the longest x4 16.7 us: with_place(): pl.pallas_call(body, grid_spec=pltpu.PrefetchScalarGridSpec(num_scalar_pr...]
    all_to_all x4 -> x5, blocking collectives: 85.2 us -> 95.4 us  [the longest x1 31.1 us: local(): lax.all_to_all(terms.reshape(16, 512, 128), TP, 0, 0, tiled=True)]
    reduce_sum x9 -> x0, other arithmetic: 8.99 us -> none  [the longest x1 5.38 us: over_pieces(): return blocks.sum(axis=0)]
    dot_general x12 -> x0, matrix products: 8.43 us -> none  [the longest x2 1.68 us: visit_block(): jnp.einsum('qhd,khd->hqk', queries, key_block, preferred_element_type=jnp...]
    reshape x3 -> x0, local copies, waits for them, and re-layouts: 4.61 us -> none  [the longest x2 3.16 us: split_heads(): return array.reshape(array.shape[0], array.shape[1] // head_size, head_size)]
  transfers between devices with their start and end apart: 4 -> 12, of which waited for: 4 -> 7; matrix products, arithmetic and copies ran while one was open for 0% -> 0% of each run, Pallas kernels for 0% -> 1%
where the time goes in v1:
time: 222 us; the launch traced here: 218 us
  blocking collectives  95.4 us (43%)
  waiting for transfers between devices  45.7 us (21%)
  starting transfers between devices  45.2 us (20%)
  Pallas kernels  19.8 us (9%)
  local copies, waits for them, and re-layouts  11.8 us (5%)
    all_to_all x1, blocking collectives, local(): lax.all_to_all(terms.reshape(16, 512, 128), TP, 0, 0, tiled=True)  31.1 us
    all_to_all x1, blocking collectives, local(): lax.all_to_all(outgoing.reshape(16, 32, 128), ('a', 'b'), 0, 0, tiled=True)  20.5 us
    all_to_all x1, blocking collectives, local(): own = lax.all_to_all(kv, 'b', 0, 0, tiled=True)  17.2 us
    all_to_all x1, blocking collectives, local(): arrived = lax.all_to_all(partial, TP, 0, 0, tiled=True)  17 us
    ppermute x3, waiting for transfers between devices, local(): lax.ppermute(q, 'a', [(i + d, i) for i in range(4 - d)])  16.7 us
    pallas_call x4, Pallas kernels, with_place(): pl.pallas_call(body, grid_spec=pltpu.PrefetchScalarGridSpec(num_scalar_pr...  16.7 us
    ppermute x3, starting transfers between devices, local(): lax.ppermute(far[d - 1], 'a', [(i, i + d) for i in range(4 - d)])  12.1 us
    all_to_all x1, waiting for transfers between devices, local(): lax.all_to_all(jnp.broadcast_to(moved.reshape(1, 512, 128), (16, 512, 128...  12 us
  transfers between devices with their start and end apart: 12, of which 7 were waited for; matrix products, arithmetic and copies ran while one was open for 0% of the time, Pallas kernels for 1%

profile of v1, /device:TPU:1, one launch (start us, length us, event | category | flops | bytes accessed | tf_op | source)
XLA Modules:
  0.0 218.2 jit_solution(17969783148162054997)
XLA Ops:
  0.0 0.9 copy.20.ks
  0.9 0.8 copy.21.vs
  1.7 0.8 copy.22.qs
  2.6 0.7 copy.26
  3.3 0.0 copy-start.10
  3.3 0.7 copy-done.10
  4.0 0.8 copy-done.11
  4.8 0.8 copy-done.12
  5.6 0.1 shard_map.181
  5.7 17.2 %all_to_all.35.own = bf16[4,144,384]{2,1,0:T(8,128)(2,1)S(1)} all-to-all(bf16[4,144,384]{2,1,0:T(8,128)(2,1)S(1)} %get-tuple-element.14), channel_id=1, replica_groups=mesh['a'=4,'b'=4,'c'=2,'y'=4,'x'=4] {'b'}, dimensions={0} | all-to-all | bytes 884736 | tf_op jit(solution)/shard_map/all_to_all | solution.py:309
  22.9 4.6 %collective-permute-start = (bf16[4,144,384]{2,1,0:T(8,128)(2,1)S(1)}, bf16[4,144,384]{2,1,0:T(8,128)(2,1)S(1)}, u32[]{:S(2)}, u32[]{:S(2)}) collective-permute-start(bf16[4,144,384]{2,1,0:T(8,128)(2,1)S(1)} %all_to_all.35.own), channel_id=1, source_target_pairs={{0,16},{16,0},{1,17},{17,1},{2,18},{18,2},{3,19},{19,3},{4,20},{20... | collective-permute-start | bytes 1327112 | tf_op jit(solution)/shard_map/ppermute | solution.py:310
  27.5 1.3 collective-permute-start.1
  28.8 1.3 collective-permute-start.2
  30.1 1.3 collective-permute-start.3
  31.4 0.1 pad_add_fusion.place
  31.5 11.5 %collective-permute-done.1.q1 = bf16[128,256]{1,0:T(8,128)(2,1)S(1)} collective-permute-done((bf16[128,256]{1,0:T(8,128)(2,1)S(1)}, bf16[128,256]{1,0:T(8,128)(2,1)S(1)}, u32[]{:S(2)}, u32[]{:S(2)}) %collective-permute-start.1) | collective-permute-done | bytes 65568 | tf_op jit(solution)/shard_map/ppermute | solution.py:308
  43.0 1.8 collective-permute-done.2.q2
  44.9 3.4 %collective-permute-done.3.q3 = bf16[128,256]{1,0:T(8,128)(2,1)S(1)} collective-permute-done((bf16[128,256]{1,0:T(8,128)(2,1)S(1)}, bf16[128,256]{1,0:T(8,128)(2,1)S(1)}, u32[]{:S(2)}, u32[]{:S(2)}) %collective-permute-start.3) | collective-permute-done | bytes 65568 | tf_op jit(solution)/shard_map/ppermute | solution.py:308
  48.3 0.0 collective-permute-done.other
  48.3 4.6 %shard_map.183 = (bf16[128,256]{1,0:T(8,128)(2,1)S(1)}, bf16[128,256]{1,0:T(8,128)(2,1)S(1)}, bf16[128,256]{1,0:T(8,128)(2,1)S(1)}) custom-call(s32[4]{0:T(128)S(1)} %pad_add_fusion.place, bf16[128,256]{1,0:T(8,128)(2,1)S(1)} %collective-permute-done.1.q1, bf16[128,256]{1,0:T(8,128)(2,1)S(1)} %collective-permute-done.2.q2, ...), custom_call_target="tpu_custom_call" | custom-call | tf_op jit(solution)/shard_map/pallas_call | solution.py:259
  52.9 0.0 copy-start.8
  52.9 0.0 copy-start.17
  52.9 7.8 %collective-permute-start.4 = (bf16[128,256]{1,0:T(8,128)(2,1)S(1)}, bf16[128,256]{1,0:T(8,128)(2,1)S(1)}, u32[]{:S(2)}, u32[]{:S(2)}) collective-permute-start(bf16[128,256]{1,0:T(8,128)(2,1)S(1)} %get-tuple-element.15), channel_id=1, source_target_pairs={{0,128},{128,256},{256,384},{1,129},{129,257},{257,385},{2,130},{1... | collective-permute-start | bytes 196616 | tf_op jit(solution)/shard_map/ppermute | solution.py:317
  60.7 3.0 %collective-permute-start.5 = (bf16[128,256]{1,0:T(8,128)(2,1)S(1)}, bf16[128,256]{1,0:T(8,128)(2,1)S(1)}, u32[]{:S(2)}, u32[]{:S(2)}) collective-permute-start(bf16[128,256]{1,0:T(8,128)(2,1)S(1)} %get-tuple-element.16), channel_id=1, source_target_pairs={{0,256},{128,384},{1,257},{129,385},{2,258},{130,386},{3,259},{131... | collective-permute-start | bytes 196616 | tf_op jit(solution)/shard_map/ppermute | solution.py:317
  63.7 1.3 collective-permute-start.6
  65.0 3.1 %shard_map.182.o0 = f32[128,256]{1,0:T(8,128)S(1)} custom-call(s32[4]{0:T(128)S(1)} %pad_add_fusion.place, bf16[128,256]{1,0:T(8,128)(2,1)S(1)} %get-tuple-element.13.q, bf16[4,144,384]{2,1,0:T(8,128)(2,1)S(1)} %all_to_all.35.own, bf16[4,144,384]{2,1,0:T(8,128)(2,1)S(1)} %collective-permute-done.other), custom_call_target="tpu_custom_call" | custom-call | tf_op jit(solution)/shard_map/pallas_call | solution.py:259
  68.2 0.0 collective-permute-done.4.o1
  68.2 0.0 collective-permute-done.5.o2
  68.2 4.8 %collective-permute-done.6.o3 = bf16[128,256]{1,0:T(8,128)(2,1)S(1)} collective-permute-done((bf16[128,256]{1,0:T(8,128)(2,1)S(1)}, bf16[128,256]{1,0:T(8,128)(2,1)S(1)}, u32[]{:S(2)}, u32[]{:S(2)}) %collective-permute-start.6) | collective-permute-done | bytes 65568 | tf_op jit(solution)/shard_map/ppermute | solution.py:317
  73.0 0.0 copy-done.9
  73.0 0.0 copy-done.7
  73.0 0.7 shard_map.184
  73.7 17.0 %all_to_all.36.arrived = bf16[16,128,128]{2,1,0:T(8,128)(2,1)S(1)} all-to-all(bf16[16,128,128]{2,1,0:T(8,128)(2,1)S(1)} %shard_map.184), channel_id=1, replica_groups=mesh['a'=4,'b'=4,'c'=2,'y'=4,'x'=4] {'y','x'}, dimensions={0} | all-to-all | bytes 1048576 | tf_op jit(solution)/shard_map/all_to_all | solution.py:321
  90.7 0.0 copy-done.8
  90.7 0.0 copy-done.17
  90.7 0.9 shard_map.185
  91.6 20.5 %all_to_all.37 = bf16[16,32,128]{2,1,0:T(8,128)(2,1)S(1)} all-to-all(bf16[16,32,128]{2,1,0:T(8,128)(2,1)S(1)} %bitcast.32), channel_id=1, replica_groups=mesh['a'=4,'b'=4,'c'=2,'y'=4,'x'=4] {'a','b'}, dimensions={0} | all-to-all | bytes 262144 | tf_op jit(solution)/shard_map/all_to_all | solution.py:328
  112.1 1.7 broadcast_in_dim.17
  113.9 0.0 copy-start.14
  113.9 4.7 %all-to-all-start.3 = ((bf16[16,512,128]{2,1,0:T(8,128)(2,1)}), bf16[16,512,128]{2,1,0:T(8,128)(2,1)}, u32[]{:S(2)}, u32[]{:S(2)}) async-start(bf16[16,512,128]{2,1,0:T(8,128)(2,1)} %broadcast_in_dim.17), calls=%async_computation.3 | async-start | bytes 4194304 | tf_op jit(solution)/shard_map/all_to_all | solution.py:329
  118.6 0.0 copy-done
  118.6 6.1 %collective-permute-start.7 = (bf16[2048,256]{1,0:T(8,128)(2,1)S(1)}, bf16[2048,256]{1,0:T(8,128)(2,1)S(1)}, u32[]{:S(2)}, u32[]{:S(2)}) collective-permute-start(bf16[2048,256]{1,0:T(8,128)(2,1)S(1)} %bitcast.25), channel_id=1, source_target_pairs={{0,16},{16,0},{1,17},{17,1},{2,18},{18,2},{3,19},{19,3},{4,20},{20... | collective-permute-start | bytes 3145736 | tf_op jit(solution)/shard_map/ppermute | solution.py:332
  124.7 0.0 copy-done.1
  124.7 1.9 collective-permute-start.8
  126.6 2.6 %collective-permute-start.9 = (bf16[256,2048]{1,0:T(8,128)(2,1)S(1)}, bf16[256,2048]{1,0:T(8,128)(2,1)}, u32[]{:S(2)}, u32[]{:S(2)}) collective-permute-start(bf16[256,2048]{1,0:T(8,128)(2,1)S(1)} %bitcast.29), channel_id=1, source_target_pairs={{0,16},{16,0},{1,17},{17,1},{2,18},{18,2},{3,19},{19,3},{4,20},{20... | collective-permute-start | bytes 3145736 | tf_op jit(solution)/shard_map/ppermute | solution.py:332
  129.2 0.0 collective-permute-done.7.gate1
  129.2 1.0 copy-done.3
  130.2 0.0 collective-permute-done.8.up1
  130.2 1.0 copy-done.5
  131.2 0.2 collective-permute-done.9.down1
  131.4 12.0 %all-to-all-done.3.rows = bf16[16,512,128]{2,1,0:T(8,128)(2,1)} async-done(((bf16[16,512,128]{2,1,0:T(8,128)(2,1)}), bf16[16,512,128]{2,1,0:T(8,128)(2,1)}, u32[]{:S(2)}, u32[]{:S(2)}) %all-to-all-start.3) | async-done | bytes 2097184 | tf_op jit(solution)/shard_map/all_to_all | solution.py:329
  143.5 0.0 copy-done.14
  143.5 1.2 copy-done.4
  144.7 1.2 copy-done.6
  145.9 8.1 %shard_map.186 = bf16[16,16,2,16,128]{4,3,2,1,0:T(8,128)(2,1)} custom-call(s32[4]{0:T(128)S(1)} %pad_add_fusion.place, bf16[16,512,128]{2,1,0:T(8,128)(2,1)} %all-to-all-done.3.rows, f32[1,2048]{1,0:T(1,128)S(1)} %bitcast.33, f32[1,2048]{1,0:T(1,128)S(1)} %bitcast.35, bf16[2048,256]{1,0:T(8,128)(2,1)S(1)} %bitcast.26, bf16[2048,256]{1,0:T(8,128)(2,1)S(1)} %bitcast.28, ...), custom_call_target="tpu_custom_call" | custom-call | tf_op jit(solution)/shard_map/pallas_call | solution.py:259
  154.1 31.1 %all_to_all.38.arrived = bf16[16,512,128]{2,1,0:T(8,128)(2,1)S(1)} all-to-all(bf16[16,512,128]{2,1,0:T(8,128)(2,1)} %bitcast.40), channel_id=1, replica_groups=mesh['a'=4,'b'=4,'c'=2,'y'=4,'x'=4] {'y','x'}, dimensions={0} | all-to-all | bytes 4194304 | tf_op jit(solution)/shard_map/all_to_all | solution.py:340
  185.2 0.9 shard_map.187
  186.2 9.3 %all-to-all-start.5 = ((bf16[16,32,128]{2,1,0:T(8,128)(2,1)}), bf16[16,32,128]{2,1,0:T(8,128)(2,1)S(1)}, u32[]{:S(2)}, u32[]{:S(2)}) async-start(bf16[16,32,128]{2,1,0:T(8,128)(2,1)} %bitcast.15), calls=%async_computation.5 | async-start | bytes 262144 | tf_op jit(solution)/shard_map/all_to_all | solution.py:342
  195.5 0.0 copy-done.18
  195.5 0.1 copy.23.weight
  195.6 11.8 %all-to-all-done.5 = bf16[16,32,128]{2,1,0:T(8,128)(2,1)S(1)} async-done(((bf16[16,32,128]{2,1,0:T(8,128)(2,1)}), bf16[16,32,128]{2,1,0:T(8,128)(2,1)S(1)}, u32[]{:S(2)}, u32[]{:S(2)}) %all-to-all-start.5) | async-done | bytes 131104 | tf_op jit(solution)/shard_map/all_to_all | solution.py:342
  207.4 0.3 shard_map.188
  207.7 9.5 %all_to_all.39.arrived = bf16[16,8,256]{2,1,0:T(8,128)(2,1)S(1)} all-to-all(bf16[16,8,256]{2,1,0:T(8,128)(2,1)S(1)} %shard_map.188), channel_id=1, replica_groups=mesh['a'=4,'b'=4,'c'=2,'y'=4,'x'=4] {'y','x'}, dimensions={0} | all-to-all | bytes 131072 | tf_op jit(solution)/shard_map/all_to_all | solution.py:346
  217.2 1.0 shard_map.189
  (21 shorter events, 0.1 us)
Async XLA Ops:
  0.0 73.0 %copy-start.9 = (bf16[64,2048]{1,0:T(8,128)(2,1)S(1)}, bf16[64,2048]{1,0:T(8,128)(2,1)}, u32[]{:S(2)}) copy-start(bf16[64,2048]{1,0:T(8,128)(2,1)} %w_small.1) | copy-start | bytes 786436
  0.0 73.0 %copy-start.7 = (bf16[128,2048]{1,0:T(8,128)(2,1)S(1)}, bf16[128,2048]{1,0:T(8,128)(2,1)}, u32[]{:S(2)}) copy-start(bf16[128,2048]{1,0:T(8,128)(2,1)} %w_large.1) | copy-start | bytes 1572868
  3.3 0.8 copy-start.10
  4.0 0.8 copy-start.11
  4.8 0.8 copy-start.12
  22.9 25.3 %collective-permute-start = (bf16[4,144,384]{2,1,0:T(8,128)(2,1)S(1)}, bf16[4,144,384]{2,1,0:T(8,128)(2,1)S(1)}, u32[]{:S(2)}, u32[]{:S(2)}) collective-permute-start(bf16[4,144,384]{2,1,0:T(8,128)(2,1)S(1)} %all_to_all.35.own), channel_id=1, source_target_pairs={{0,16},{16,0},{1,17},{17,1},{2,18},{18,2},{3,19},{19,3},{4,20},{20... | collective-permute-start | bytes 1327112 | tf_op jit(solution)/shard_map/ppermute | solution.py:310
  27.5 15.5 %collective-permute-start.1 = (bf16[128,256]{1,0:T(8,128)(2,1)S(1)}, bf16[128,256]{1,0:T(8,128)(2,1)S(1)}, u32[]{:S(2)}, u32[]{:S(2)}) collective-permute-start(bf16[128,256]{1,0:T(8,128)(2,1)S(1)} %get-tuple-element.13.q), channel_id=1, source_target_pairs={{128,0},{256,128},{384,256},{129,1},{257,129},{385,257},{130,2},{2... | collective-permute-start | bytes 196616 | tf_op jit(solution)/shard_map/ppermute | solution.py:308
  28.8 16.1 %collective-permute-start.2 = (bf16[128,256]{1,0:T(8,128)(2,1)S(1)}, bf16[128,256]{1,0:T(8,128)(2,1)S(1)}, u32[]{:S(2)}, u32[]{:S(2)}) collective-permute-start(bf16[128,256]{1,0:T(8,128)(2,1)S(1)} %get-tuple-element.13.q), channel_id=1, source_target_pairs={{256,0},{384,128},{257,1},{385,129},{258,2},{386,130},{259,3},{387... | collective-permute-start | bytes 196616 | tf_op jit(solution)/shard_map/ppermute | solution.py:308
  30.1 18.1 %collective-permute-start.3 = (bf16[128,256]{1,0:T(8,128)(2,1)S(1)}, bf16[128,256]{1,0:T(8,128)(2,1)S(1)}, u32[]{:S(2)}, u32[]{:S(2)}) collective-permute-start(bf16[128,256]{1,0:T(8,128)(2,1)S(1)} %get-tuple-element.13.q), channel_id=1, source_target_pairs={{384,0},{385,1},{386,2},{387,3},{388,4},{389,5},{390,6},{391,7},{3... | collective-permute-start | bytes 196616 | tf_op jit(solution)/shard_map/ppermute | solution.py:308
  52.9 37.9 %copy-start.8 = (bf16[128,2048]{1,0:T(8,128)(2,1)S(1)}, bf16[128,2048]{1,0:T(8,128)(2,1)}, u32[]{:S(2)}) copy-start(bf16[128,2048]{1,0:T(8,128)(2,1)} %stream.1) | copy-start | bytes 1572868
  52.9 37.8 %copy-start.17 = (s32[128,2]{0,1:T(2,128)S(1)}, s32[128,2]{0,1:T(2,128)}, u32[]{:S(2)}) copy-start(s32[128,2]{0,1:T(2,128)} %param.33) | copy-start | bytes 3076
  52.9 15.3 %collective-permute-start.4 = (bf16[128,256]{1,0:T(8,128)(2,1)S(1)}, bf16[128,256]{1,0:T(8,128)(2,1)S(1)}, u32[]{:S(2)}, u32[]{:S(2)}) collective-permute-start(bf16[128,256]{1,0:T(8,128)(2,1)S(1)} %get-tuple-element.15), channel_id=1, source_target_pairs={{0,128},{128,256},{256,384},{1,129},{129,257},{257,385},{2,130},{1... | collective-permute-start | bytes 196616 | tf_op jit(solution)/shard_map/ppermute | solution.py:317
  60.7 7.5 %collective-permute-start.5 = (bf16[128,256]{1,0:T(8,128)(2,1)S(1)}, bf16[128,256]{1,0:T(8,128)(2,1)S(1)}, u32[]{:S(2)}, u32[]{:S(2)}) collective-permute-start(bf16[128,256]{1,0:T(8,128)(2,1)S(1)} %get-tuple-element.16), channel_id=1, source_target_pairs={{0,256},{128,384},{1,257},{129,385},{2,258},{130,386},{3,259},{131... | collective-permute-start | bytes 196616 | tf_op jit(solution)/shard_map/ppermute | solution.py:317
  63.7 9.2 %collective-permute-start.6 = (bf16[128,256]{1,0:T(8,128)(2,1)S(1)}, bf16[128,256]{1,0:T(8,128)(2,1)S(1)}, u32[]{:S(2)}, u32[]{:S(2)}) collective-permute-start(bf16[128,256]{1,0:T(8,128)(2,1)S(1)} %get-tuple-element.17), channel_id=1, source_target_pairs={{0,384},{1,385},{2,386},{3,387},{4,388},{5,389},{6,390},{7,391},{8... | collective-permute-start | bytes 196616 | tf_op jit(solution)/shard_map/ppermute | solution.py:317
  113.8 4.7 %copy-start = (bf16[1,2048,256]{2,1,0:T(8,128)(2,1)S(1)}, bf16[1,2048,256]{2,1,0:T(8,128)(2,1)}, u32[]{:S(2)}) copy-start(bf16[1,2048,256]{2,1,0:T(8,128)(2,1)} %param.35) | copy-start | bytes 3145732
  113.8 10.8 %copy-start.1 = (bf16[1,2048,256]{2,1,0:T(8,128)(2,1)S(1)}, bf16[1,2048,256]{2,1,0:T(8,128)(2,1)}, u32[]{:S(2)}) copy-start(bf16[1,2048,256]{2,1,0:T(8,128)(2,1)} %param.36) | copy-start | bytes 3145732
  113.8 12.8 %copy-start.2 = (bf16[1,256,2048]{2,1,0:T(8,128)(2,1)S(1)}, bf16[1,256,2048]{2,1,0:T(8,128)(2,1)}, u32[]{:S(2)}) copy-start(bf16[1,256,2048]{2,1,0:T(8,128)(2,1)} %param.37) | copy-start | bytes 3145732
  113.8 29.6 %copy-start.13 = (f32[2048]{0:T(1024)S(1)}, f32[2048]{0:T(1024)}, u32[]{:S(2)}) copy-start(f32[2048]{0:T(1024)} %param.29) | copy-start | bytes 24580
  113.9 29.6 %copy-start.14 = (f32[2048]{0:T(1024)S(1)}, f32[2048]{0:T(1024)}, u32[]{:S(2)}) copy-start(f32[2048]{0:T(1024)} %param.30) | copy-start | bytes 24580
  113.9 29.6 %all-to-all-start.3 = ((bf16[16,512,128]{2,1,0:T(8,128)(2,1)}), bf16[16,512,128]{2,1,0:T(8,128)(2,1)}, u32[]{:S(2)}, u32[]{:S(2)}) async-start(bf16[16,512,128]{2,1,0:T(8,128)(2,1)} %broadcast_in_dim.17), calls=%async_computation.3 | async-start | bytes 4194304 | tf_op jit(solution)/shard_map/all_to_all | solution.py:329
  118.6 10.6 %collective-permute-start.7 = (bf16[2048,256]{1,0:T(8,128)(2,1)S(1)}, bf16[2048,256]{1,0:T(8,128)(2,1)S(1)}, u32[]{:S(2)}, u32[]{:S(2)}) collective-permute-start(bf16[2048,256]{1,0:T(8,128)(2,1)S(1)} %bitcast.25), channel_id=1, source_target_pairs={{0,16},{16,0},{1,17},{17,1},{2,18},{18,2},{3,19},{19,3},{4,20},{20... | collective-permute-start | bytes 3145736 | tf_op jit(solution)/shard_map/ppermute | solution.py:332
  124.7 5.5 %collective-permute-start.8 = (bf16[2048,256]{1,0:T(8,128)(2,1)S(1)}, bf16[2048,256]{1,0:T(8,128)(2,1)S(1)}, u32[]{:S(2)}, u32[]{:S(2)}) collective-permute-start(bf16[2048,256]{1,0:T(8,128)(2,1)S(1)} %bitcast.27), channel_id=1, source_target_pairs={{0,16},{16,0},{1,17},{17,1},{2,18},{18,2},{3,19},{19,3},{4,20},{20... | collective-permute-start | bytes 3145736 | tf_op jit(solution)/shard_map/ppermute | solution.py:332
  126.6 4.8 %collective-permute-start.9 = (bf16[256,2048]{1,0:T(8,128)(2,1)S(1)}, bf16[256,2048]{1,0:T(8,128)(2,1)}, u32[]{:S(2)}, u32[]{:S(2)}) collective-permute-start(bf16[256,2048]{1,0:T(8,128)(2,1)S(1)} %bitcast.29), channel_id=1, source_target_pairs={{0,16},{16,0},{1,17},{17,1},{2,18},{18,2},{3,19},{19,3},{4,20},{20... | collective-permute-start | bytes 3145736 | tf_op jit(solution)/shard_map/ppermute | solution.py:332
  129.2 1.0 copy-start.3
  130.2 1.0 copy-start.5
  143.5 1.2 copy-start.4
  144.7 1.2 copy-start.6
  185.2 10.2 %copy-start.18 = (f32[128,2]{0,1:T(2,128)S(1)}, f32[128,2]{0,1:T(2,128)}, u32[]{:S(2)}) copy-start(f32[128,2]{0,1:T(2,128)} %param.34) | copy-start | bytes 3076
  185.2 32.0 %copy-start.15 = (f32[2048]{0:T(1024)S(1)}, f32[2048]{0:T(1024)}, u32[]{:S(2)}) copy-start(f32[2048]{0:T(1024)} %param.31) | copy-start | bytes 24580
  185.2 32.0 %copy-start.16 = (f32[2048]{0:T(1024)S(1)}, f32[2048]{0:T(1024)}, u32[]{:S(2)}) copy-start(f32[2048]{0:T(1024)} %param.32) | copy-start | bytes 24580
  186.2 21.3 %all-to-all-start.5 = ((bf16[16,32,128]{2,1,0:T(8,128)(2,1)}), bf16[16,32,128]{2,1,0:T(8,128)(2,1)S(1)}, u32[]{:S(2)}, u32[]{:S(2)}) async-start(bf16[16,32,128]{2,1,0:T(8,128)(2,1)} %bitcast.15), calls=%async_computation.5 | async-start | bytes 262144 | tf_op jit(solution)/shard_map/all_to_all | solution.py:342
